TPU v7x, 32 devices: a whole 2x2x4 slice. The times are simulated.
32 devices in a mesh: dp: 4 (over y, x), kv: 4 (over z), tp: 2 (over core).
Axes of the slice: x: 2, y: 2, z: 4, core: 2. Of those that a mesh axis runs over, the one named last changes fastest.
Arguments:
- tokens: bfloat16 [4096, 2048], P(('dp', 'kv'), 'tp'), parts along dimension 0, may hold values from -6 to 6
- query_weight: bfloat16 [2048, 1024], P(None, 'tp'), may hold values from -2 to 2
- key_weight: bfloat16 [2048, 1024], P(None, 'tp'), may hold values from -2 to 2
- value_weight: bfloat16 [2048, 1024], P(None, 'tp'), may hold values from -0.125 to 0.125
- out_weight: bfloat16 [1024, 2048], P(None, 'tp'), may hold values from -0.75 to 0.75
- chosen: int32 [128, 16], P(('dp', 'kv')), parts along dimension 0, may hold values from -1 to 31, as said below
Outputs:
- mixed: bfloat16 [4096, 2048], P(('dp', 'kv'), 'tp'), parts along dimension 0
There are 4 independent parts, one for each index of `dp`. A program takes and returns all parts, laid end to end along the dimension named above; an argument that names none is the same for every part. Nothing has to cross between parts.
Inputs may be any that keep to these rules, and one draw needn't show every extreme that they name: Each row of chosen lists distinct key blocks no later than its own query block, followed or mixed with -1 for empty slots; the own block is always listed, and block 0 too. For the 8 query blocks of one index of kv (aligned runs of rows), the distinct listed key blocks that lie among the 8 blocks of any one other index number at most 3, and exactly 3 for the index just before.
All inputs are finite; a program needn't handle non-finite values.
Results may differ from a plain program's by a relative error of at most 0.0084.
Values may be sent and summed in bfloat16 or wider, within the bound.
A program may use at most 128 MiB of HBM per device.

v0:
```python
import jax
import jax.numpy as jnp
from jax import lax
from jax.sharding import PartitionSpec as P

HEAD_DIM = 64
BLOCK = 32
CAP = 3


rotary_base = 500000.0
masked_score = -1e30


def rotate(heads_in, positions):
    half_dim = heads_in.shape[-1] // 2
    inverse = 1.0 / rotary_base ** (jnp.arange(half_dim, dtype=jnp.float32) / half_dim)
    angles = positions.astype(jnp.float32)[:, None] * inverse[None, :]
    cosine = jnp.cos(angles)[:, None, :]
    sine_part = jnp.sin(angles)[:, None, :]
    first_half = heads_in[..., :half_dim]
    second_half = heads_in[..., half_dim:]
    return jnp.concatenate(
        [
            first_half * cosine - second_half * sine_part,
            first_half * sine_part + second_half * cosine,
        ],
        axis=-1,
    )


def attend_keys(
    carried, queries, key_rows, value_rows, key_block, key_pos, key_valid, listed, query_pos
):
    key_count = key_rows.shape[0]
    head_count = queries.shape[0]
    hit_mask = jnp.any(listed[:, :, None] == key_block[None, None, :], axis=1)
    hit_mask = jnp.repeat(hit_mask, BLOCK, axis=0)
    allowed = hit_mask & key_valid[None, :] & (key_pos[None, :] <= query_pos[:, None])
    keys_heads = key_rows.reshape(key_count, head_count, HEAD_DIM).transpose(1, 0, 2)
    values_heads = value_rows.reshape(key_count, head_count, HEAD_DIM).transpose(1, 0, 2)
    score_scale = HEAD_DIM ** (-0.5)

    def one_head(inputs):
        query_head, key_head, value_head, peak_now, denominator, summed = inputs
        scores = (
            jnp.einsum("qd,kd->qk", query_head, key_head, preferred_element_type=jnp.float32)
            * score_scale
        )
        scores = jnp.where(allowed, scores, masked_score)
        peak_new = jnp.maximum(peak_now, jnp.max(scores, axis=1))
        factor = jnp.exp(peak_now - peak_new)
        weights = jnp.where(allowed, jnp.exp(scores - peak_new[:, None]), 0.0)
        denominator = denominator * factor + jnp.sum(weights, axis=1)
        summed = summed * factor[:, None] + jnp.dot(
            weights.astype(jnp.bfloat16), value_head, preferred_element_type=jnp.float32
        )
        return (peak_new, denominator, summed)

    peak_now, denominator, summed = carried
    return lax.map(one_head, (queries, keys_heads, values_heads, peak_now, denominator, summed))


def on_device(tokens, query_weight, key_weight, value_weight, out_weight, chosen):
    row_count = tokens.shape[0]
    head_width = query_weight.shape[1]
    head_count = head_width // HEAD_DIM
    device = lax.axis_index("kv")
    devices = lax.axis_size("kv")
    blocks_dev = row_count // BLOCK
    query_pos = device * row_count + jnp.arange(row_count, dtype=jnp.int32)
    fragment = lax.all_gather(tokens, "tp", axis=1, tiled=True)
    query_acc, key_acc, value_acc = tuple(
        (
            jnp.dot(fragment, weight, preferred_element_type=jnp.float32)
            for weight in (query_weight, key_weight, value_weight)
        )
    )
    heads_shape = (row_count, head_count, HEAD_DIM)
    query_proj = rotate(query_acc.reshape(heads_shape), query_pos).astype(jnp.bfloat16)
    key_proj = (
        rotate(key_acc.reshape(heads_shape), query_pos)
        .astype(jnp.bfloat16)
        .reshape(row_count, head_width)
    )
    value_proj = value_acc.astype(jnp.bfloat16)
    queries = query_proj.transpose(1, 0, 2)
    start_state = (
        jnp.full((head_count, row_count), masked_score, jnp.float32),
        jnp.zeros((head_count, row_count), jnp.float32),
        jnp.zeros((head_count, row_count, HEAD_DIM), jnp.float32),
    )
    block_ids = jnp.arange(devices * blocks_dev, dtype=jnp.int32)
    needed = jnp.any(chosen.reshape(-1)[:, None] == block_ids[None, :], axis=0)
    needed = needed & (block_ids // blocks_dev != device)
    need_grid = needed.reshape(devices, blocks_dev).astype(jnp.int32)
    rank_in = jnp.cumsum(need_grid, axis=1) - need_grid
    slot_hit = (need_grid[:, None, :] == 1) & (
        rank_in[:, None, :] == jnp.arange(CAP, dtype=jnp.int32)[None, :, None]
    )
    request = jnp.sum(
        slot_hit.astype(jnp.int32) * jnp.arange(blocks_dev, dtype=jnp.int32)[None, None, :], axis=2
    )
    present = jnp.any(slot_hit, axis=2)
    incoming = lax.all_to_all(request, "kv", split_axis=0, concat_axis=0, tiled=True)
    key_store = key_proj.reshape(blocks_dev, BLOCK, head_width)
    value_store = value_proj.reshape(blocks_dev, BLOCK, head_width)
    got_keys, got_values = (
        lax.all_to_all(key_store[incoming], "kv", split_axis=0, concat_axis=0, tiled=True),
        lax.all_to_all(value_store[incoming], "kv", split_axis=0, concat_axis=0, tiled=True),
    )
    remote_block = jnp.arange(devices, dtype=jnp.int32)[:, None] * blocks_dev + request
    remote_pos = (
        remote_block[:, :, None] * BLOCK + jnp.arange(BLOCK, dtype=jnp.int32)[None, None, :]
    ).reshape(-1)
    remote_valid = jnp.broadcast_to(present[:, :, None], (devices, CAP, BLOCK)).reshape(-1)
    key_rows = jnp.concatenate([key_proj, got_keys.reshape(-1, head_width)], axis=0)
    value_rows = jnp.concatenate([value_proj, got_values.reshape(-1, head_width)], axis=0)
    key_pos = jnp.concatenate([query_pos, remote_pos])
    key_valid = jnp.concatenate([jnp.ones((row_count,), jnp.bool_), remote_valid])
    peak_now, denominator, summed = attend_keys(
        start_state,
        queries,
        key_rows,
        value_rows,
        key_pos // BLOCK,
        key_pos,
        key_valid,
        chosen,
        query_pos,
    )
    attended = (
        (summed / denominator[:, :, None])
        .astype(jnp.bfloat16)
        .transpose(1, 0, 2)
        .reshape(row_count, head_width)
    )
    mixed = jnp.dot(
        lax.all_gather(attended, "tp", axis=1, tiled=True),
        out_weight,
        preferred_element_type=jnp.float32,
    )
    return mixed.astype(jnp.bfloat16)


def solution(mesh):
    placed = (
        P(("dp", "kv"), "tp"),
        P(None, "tp"),
        P(None, "tp"),
        P(None, "tp"),
        P(None, "tp"),
        P(("dp", "kv"), None),
    )
    return jax.shard_map(
        on_device, mesh=mesh, in_specs=placed, out_specs=P(("dp", "kv"), "tp"), check_vma=False
    )
```

profile of v0, /device:TPU:0, one launch (start us, length us, event | category | flops | bytes accessed | tf_op | source)
XLA Modules:
  0.0 97.7 jit_solution(7026933683414445117)
XLA Ops:
  6.5 0.7 all-gather.2.cloned.1.call-update
  7.3 0.8 eq.50
  8.6 0.7 copy.41
  9.3 6.3 %all-to-all-start = ((s32[4,1,3]{2,1,0:T(1,128)}), s32[4,1,3]{2,1,0:T(1,128)S(1)}, u32[]{:S(2)}, u32[]{:S(2)}) async-start(s32[4,1,3]{2,1,0:T(1,128)} %copy.41), calls=%async_computation | async-start | bytes 4096 | tf_op jit(solution)/shard_map/all_to_all | solution.py:105
  16.0 5.1 %all-to-all-done = s32[4,1,3]{2,1,0:T(1,128)S(1)} async-done(((s32[4,1,3]{2,1,0:T(1,128)}), s32[4,1,3]{2,1,0:T(1,128)S(1)}, u32[]{:S(2)}, u32[]{:S(2)}) %all-to-all-start) | async-done | bytes 80 | tf_op jit(solution)/shard_map/all_to_all | solution.py:105
  21.4 2.8 %fusion.36 = f32[256,512]{0,1:T(8,128)S(1)} fusion(bf16[256,2048]{1,0:T(8,128)(2,1)} %all-gather.2.cloned.1.call-done, bf16[2048,512]{1,0:T(8,128)(2,1)} %param.10), kind=kOutput, calls=%fused_computation.78 | convolution fusion | flops 536870912 | bytes 3670016 | tf_op jit(solution)/shard_map/dot_general | solution.py:75
  25.1 1.3 %gather_fusion = bf16[12,32,512]{2,1,0:T(8,128)(2,1)} fusion(bf16[8,32,512]{2,1,0:T(8,128)(2,1)S(1)} %convert_element_type.47, s32[1024]{0:T(1024)S(1)} %pad_clamp_fusion), kind=kCustom, calls=%fused_computation | custom fusion | bytes 786480 | tf_op jit(solution)/shard_map/gather | solution.py:109
  26.4 4.1 %all-to-all-start.1 = ((bf16[4,3,32,512]{3,2,1,0:T(8,128)(2,1)}), bf16[4,3,32,512]{3,2,1,0:T(8,128)(2,1)S(1)}, u32[]{:S(2)}, u32[]{:S(2)}) async-start(bf16[4,3,32,512]{3,2,1,0:T(8,128)(2,1)} %bitcast.5), calls=%async_computation.1 | async-start | bytes 786432 | tf_op jit(solution)/shard_map/all_to_all | solution.py:109
  31.0 0.6 concatenate.45
  31.8 2.6 %convolution_convert_fusion.1 = bf16[256,512]{1,0:T(8,128)(2,1)S(1)} fusion(bf16[256,2048]{1,0:T(8,128)(2,1)} %all-gather.2.cloned.1.call-done, bf16[2048,512]{1,0:T(8,128)(2,1)} %param.11), kind=kOutput, calls=%fused_computation.30 | convolution fusion | flops 537001984 | bytes 3407872 | tf_op jit(solution)/shard_map/dot_general | solution.py:75
  34.4 1.3 %gather_fusion.1 = bf16[12,32,512]{2,1,0:T(8,128)(2,1)} fusion(bf16[8,32,512]{2,1,0:T(8,128)(2,1)S(1)} %bitcast.71, s32[1024]{0:T(1024)S(1)} %pad_clamp_fusion), kind=kCustom, calls=%fused_computation.1 | custom fusion | bytes 786480 | tf_op jit(solution)/shard_map/gather | solution.py:110
  35.8 6.9 %all-to-all-done.1 = bf16[4,3,32,512]{3,2,1,0:T(8,128)(2,1)S(1)} async-done(((bf16[4,3,32,512]{3,2,1,0:T(8,128)(2,1)}), bf16[4,3,32,512]{3,2,1,0:T(8,128)(2,1)S(1)}, u32[]{:S(2)}, u32[]{:S(2)}) %all-to-all-start.1) | async-done | bytes 393248 | tf_op jit(solution)/shard_map/all_to_all | solution.py:109
  42.7 4.1 %all-to-all-start.2 = ((bf16[4,3,32,512]{3,2,1,0:T(8,128)(2,1)}), bf16[4,3,32,512]{3,2,1,0:T(8,128)(2,1)}, u32[]{:S(2)}, u32[]{:S(2)}) async-start(bf16[4,3,32,512]{3,2,1,0:T(8,128)(2,1)} %bitcast.9), calls=%async_computation.2 | async-start | bytes 786432 | tf_op jit(solution)/shard_map/all_to_all | solution.py:110
  46.8 3.6 %fusion.35 = f32[256,512]{0,1:T(8,128)} fusion(bf16[256,2048]{1,0:T(8,128)(2,1)} %all-gather.2.cloned.1.call-done, bf16[2048,512]{1,0:T(8,128)(2,1)} %param.9), kind=kOutput, calls=%fused_computation.77 | convolution fusion | flops 536870912 | bytes 3670016 | tf_op jit(solution)/shard_map/dot_general | solution.py:75
  50.6 1.1 %copy.46 = bf16[256,8,64]{2,1,0:T(8,128)(2,1)} copy(bf16[256,8,64]{0,2,1:T(8,128)(2,1)S(1)} %bitcast.73) | data formatting | bytes 524288 | tf_op jit(solution)/shard_map/concatenate | solution.py:118
  51.6 1.1 %subtract_convert_fusion = (bf16[256,8,32]{0,2,1:T(8,128)(2,1)S(1)}, bf16[256,8,32]{0,2,1:T(8,128)(2,1)S(1)}) fusion(f32[256,8,64]{0,2,1:T(8,128)} %bitcast.74, f32[256,32]{0,1:T(8,128)} %copy-done.5, f32[256,32]{0,1:T(8,128)} %copy-done.4), kind=kLoop, calls=%fused_computation.38 | loop fusion | flops 524288 | bytes 851968 | tf_op jit(solution)/shard_map/convert
  52.8 0.7 maximum_bitcast_fusion.2
  53.5 1.5 %concatenate.42 = bf16[384,8,64]{2,1,0:T(8,128)(2,1)S(1)} reshape(bf16[4,3,32,512]{3,2,1,0:T(8,128)(2,1)} %copy-done.2) | data formatting | bytes 786432 | tf_op jit(solution)/shard_map/concatenate | solution.py:117
  55.3 1.3 %copy.50 = bf16[8,640,64]{2,1,0:T(8,128)(2,1)} copy(bf16[8,640,64]{2,0,1:T(8,128)(2,1)S(1)} %maximum_bitcast_fusion) | data formatting | bytes 1310720
  56.6 1.6 %all-to-all-done.2 = bf16[4,3,32,512]{3,2,1,0:T(8,128)(2,1)} async-done(((bf16[4,3,32,512]{3,2,1,0:T(8,128)(2,1)}), bf16[4,3,32,512]{3,2,1,0:T(8,128)(2,1)}, u32[]{:S(2)}, u32[]{:S(2)}) %all-to-all-start.2) | async-done | bytes 393248 | tf_op jit(solution)/shard_map/all_to_all | solution.py:110
  58.1 1.5 %concatenate.47 = bf16[384,8,64]{2,1,0:T(8,128)(2,1)S(1)} reshape(bf16[4,3,32,512]{3,2,1,0:T(8,128)(2,1)} %all-to-all-done.2) | data formatting | bytes 786432 | tf_op jit(solution)/shard_map/concatenate | solution.py:118
  60.0 1.3 %copy.51 = bf16[8,640,64]{2,1,0:T(8,128)(2,1)} copy(bf16[8,640,64]{2,0,1:T(8,128)(2,1)S(1)} %maximum_bitcast_fusion.1) | data formatting | bytes 1310720
  61.3 25.8 %while.13 = (s32[]{:T(128)}, f32[8,256]{1,0:T(8,128)S(1)}, f32[8,256,64]{1,2,0:T(8,128)S(1)}, bf16[8,256,64]{1,2,0:T(8,128)(2,1)}, bf16[8,640,64]{2,1,0:T(8,128)...) while((s32[]{:T(128)}, f32[8,256]{1,0:T(8,128)S(1)}, ...), condition=%wide.region_8.9_spmd.clone, body=%wide.region_5.8_spmd.clone.sunk | while | flops 44417792 | bytes 2917761 | solution.py:61
  61.5 1.3 %fusion.54 = (f32[256]{0:T(256)S(1)}, f32[256,640]{1,0:T(8,128)S(1)}) fusion(pred[256,640]{1,0:T(32,128)(4,1)S(1)} %fusion.53, bf16[8,640,64]{2,1,0:T(8,128)(2,1)} %get-tuple-element.234, s32[]{:T(128)S(6)} %copy.62, bf16[8,256,64]{1,2,0:T(8,128)(2,1)} %get-tuple-element.233), kind=kOutput, calls=%fused_computation.76.clone.1 | convolution fusion | flops 21462784 | bytes 1017856 | tf_op jit(solution)/shard_map/while/body/eval_jaxpr/qd,kd->qk/dot_general | solution.py:47
  62.8 0.4 fusion.55
  63.2 1.3 %fusion.56 = f32[8,256,64]{1,2,0:T(8,128)S(1)} fusion(f32[8,256,64]{1,2,0:T(8,128)S(1)} %get-tuple-element.220, s32[]{:T(128)S(6)} %copy.62, pred[256,640]{1,0:T(32,128)(4,1)S(1)} %fusion.53, f32[256,640]{1,0:T(8,128)S(1)} %get-tuple-element.203, f32[256]{0:T(256)S(1)} %broadcast_maximum_fusion.2, bf16[8,640,64]{2,1,0:T(8,128)(2,1)} %get-tuple-element.235, ...), kind=kOutput, calls=%fused_computation.7.clone.1 | convolution fusion | flops 21479424 | bytes 1051648 | tf_op jit(solution)/shard_map/while/body/eval_jaxpr/dot_general | solution.py:55
  64.7 1.3 %fusion.54 = (f32[256]{0:T(256)S(1)}, f32[256,640]{1,0:T(8,128)S(1)}) fusion(pred[256,640]{1,0:T(32,128)(4,1)S(1)} %fusion.53, bf16[8,640,64]{2,1,0:T(8,128)(2,1)} %get-tuple-element.234, s32[]{:T(128)S(6)} %copy.62, bf16[8,256,64]{1,2,0:T(8,128)(2,1)} %get-tuple-element.233), kind=kOutput, calls=%fused_computation.76.clone.1 | convolution fusion | flops 21462784 | bytes 1017856 | tf_op jit(solution)/shard_map/while/body/eval_jaxpr/qd,kd->qk/dot_general | solution.py:47
  66.0 0.4 fusion.55
  66.4 1.3 %fusion.56 = f32[8,256,64]{1,2,0:T(8,128)S(1)} fusion(f32[8,256,64]{1,2,0:T(8,128)S(1)} %get-tuple-element.220, s32[]{:T(128)S(6)} %copy.62, pred[256,640]{1,0:T(32,128)(4,1)S(1)} %fusion.53, f32[256,640]{1,0:T(8,128)S(1)} %get-tuple-element.203, f32[256]{0:T(256)S(1)} %broadcast_maximum_fusion.2, bf16[8,640,64]{2,1,0:T(8,128)(2,1)} %get-tuple-element.235, ...), kind=kOutput, calls=%fused_computation.7.clone.1 | convolution fusion | flops 21479424 | bytes 1051648 | tf_op jit(solution)/shard_map/while/body/eval_jaxpr/dot_general | solution.py:55
  67.9 1.3 %fusion.54 = (f32[256]{0:T(256)S(1)}, f32[256,640]{1,0:T(8,128)S(1)}) fusion(pred[256,640]{1,0:T(32,128)(4,1)S(1)} %fusion.53, bf16[8,640,64]{2,1,0:T(8,128)(2,1)} %get-tuple-element.234, s32[]{:T(128)S(6)} %copy.62, bf16[8,256,64]{1,2,0:T(8,128)(2,1)} %get-tuple-element.233), kind=kOutput, calls=%fused_computation.76.clone.1 | convolution fusion | flops 21462784 | bytes 1017856 | tf_op jit(solution)/shard_map/while/body/eval_jaxpr/qd,kd->qk/dot_general | solution.py:47
  69.2 0.4 fusion.55
  69.7 1.3 %fusion.56 = f32[8,256,64]{1,2,0:T(8,128)S(1)} fusion(f32[8,256,64]{1,2,0:T(8,128)S(1)} %get-tuple-element.220, s32[]{:T(128)S(6)} %copy.62, pred[256,640]{1,0:T(32,128)(4,1)S(1)} %fusion.53, f32[256,640]{1,0:T(8,128)S(1)} %get-tuple-element.203, f32[256]{0:T(256)S(1)} %broadcast_maximum_fusion.2, bf16[8,640,64]{2,1,0:T(8,128)(2,1)} %get-tuple-element.235, ...), kind=kOutput, calls=%fused_computation.7.clone.1 | convolution fusion | flops 21479424 | bytes 1051648 | tf_op jit(solution)/shard_map/while/body/eval_jaxpr/dot_general | solution.py:55
  71.1 1.3 %fusion.54 = (f32[256]{0:T(256)S(1)}, f32[256,640]{1,0:T(8,128)S(1)}) fusion(pred[256,640]{1,0:T(32,128)(4,1)S(1)} %fusion.53, bf16[8,640,64]{2,1,0:T(8,128)(2,1)} %get-tuple-element.234, s32[]{:T(128)S(6)} %copy.62, bf16[8,256,64]{1,2,0:T(8,128)(2,1)} %get-tuple-element.233), kind=kOutput, calls=%fused_computation.76.clone.1 | convolution fusion | flops 21462784 | bytes 1017856 | tf_op jit(solution)/shard_map/while/body/eval_jaxpr/qd,kd->qk/dot_general | solution.py:47
  72.5 0.4 fusion.55
  72.9 1.3 %fusion.56 = f32[8,256,64]{1,2,0:T(8,128)S(1)} fusion(f32[8,256,64]{1,2,0:T(8,128)S(1)} %get-tuple-element.220, s32[]{:T(128)S(6)} %copy.62, pred[256,640]{1,0:T(32,128)(4,1)S(1)} %fusion.53, f32[256,640]{1,0:T(8,128)S(1)} %get-tuple-element.203, f32[256]{0:T(256)S(1)} %broadcast_maximum_fusion.2, bf16[8,640,64]{2,1,0:T(8,128)(2,1)} %get-tuple-element.235, ...), kind=kOutput, calls=%fused_computation.7.clone.1 | convolution fusion | flops 21479424 | bytes 1051648 | tf_op jit(solution)/shard_map/while/body/eval_jaxpr/dot_general | solution.py:55
  74.4 1.3 %fusion.54 = (f32[256]{0:T(256)S(1)}, f32[256,640]{1,0:T(8,128)S(1)}) fusion(pred[256,640]{1,0:T(32,128)(4,1)S(1)} %fusion.53, bf16[8,640,64]{2,1,0:T(8,128)(2,1)} %get-tuple-element.234, s32[]{:T(128)S(6)} %copy.62, bf16[8,256,64]{1,2,0:T(8,128)(2,1)} %get-tuple-element.233), kind=kOutput, calls=%fused_computation.76.clone.1 | convolution fusion | flops 21462784 | bytes 1017856 | tf_op jit(solution)/shard_map/while/body/eval_jaxpr/qd,kd->qk/dot_general | solution.py:47
  75.7 0.4 fusion.55
  76.1 1.3 %fusion.56 = f32[8,256,64]{1,2,0:T(8,128)S(1)} fusion(f32[8,256,64]{1,2,0:T(8,128)S(1)} %get-tuple-element.220, s32[]{:T(128)S(6)} %copy.62, pred[256,640]{1,0:T(32,128)(4,1)S(1)} %fusion.53, f32[256,640]{1,0:T(8,128)S(1)} %get-tuple-element.203, f32[256]{0:T(256)S(1)} %broadcast_maximum_fusion.2, bf16[8,640,64]{2,1,0:T(8,128)(2,1)} %get-tuple-element.235, ...), kind=kOutput, calls=%fused_computation.7.clone.1 | convolution fusion | flops 21479424 | bytes 1051648 | tf_op jit(solution)/shard_map/while/body/eval_jaxpr/dot_general | solution.py:55
  77.6 1.3 %fusion.54 = (f32[256]{0:T(256)S(1)}, f32[256,640]{1,0:T(8,128)S(1)}) fusion(pred[256,640]{1,0:T(32,128)(4,1)S(1)} %fusion.53, bf16[8,640,64]{2,1,0:T(8,128)(2,1)} %get-tuple-element.234, s32[]{:T(128)S(6)} %copy.62, bf16[8,256,64]{1,2,0:T(8,128)(2,1)} %get-tuple-element.233), kind=kOutput, calls=%fused_computation.76.clone.1 | convolution fusion | flops 21462784 | bytes 1017856 | tf_op jit(solution)/shard_map/while/body/eval_jaxpr/qd,kd->qk/dot_general | solution.py:47
  78.9 0.4 fusion.55
  79.4 1.3 %fusion.56 = f32[8,256,64]{1,2,0:T(8,128)S(1)} fusion(f32[8,256,64]{1,2,0:T(8,128)S(1)} %get-tuple-element.220, s32[]{:T(128)S(6)} %copy.62, pred[256,640]{1,0:T(32,128)(4,1)S(1)} %fusion.53, f32[256,640]{1,0:T(8,128)S(1)} %get-tuple-element.203, f32[256]{0:T(256)S(1)} %broadcast_maximum_fusion.2, bf16[8,640,64]{2,1,0:T(8,128)(2,1)} %get-tuple-element.235, ...), kind=kOutput, calls=%fused_computation.7.clone.1 | convolution fusion | flops 21479424 | bytes 1051648 | tf_op jit(solution)/shard_map/while/body/eval_jaxpr/dot_general | solution.py:55
  80.8 1.3 %fusion.54 = (f32[256]{0:T(256)S(1)}, f32[256,640]{1,0:T(8,128)S(1)}) fusion(pred[256,640]{1,0:T(32,128)(4,1)S(1)} %fusion.53, bf16[8,640,64]{2,1,0:T(8,128)(2,1)} %get-tuple-element.234, s32[]{:T(128)S(6)} %copy.62, bf16[8,256,64]{1,2,0:T(8,128)(2,1)} %get-tuple-element.233), kind=kOutput, calls=%fused_computation.76.clone.1 | convolution fusion | flops 21462784 | bytes 1017856 | tf_op jit(solution)/shard_map/while/body/eval_jaxpr/qd,kd->qk/dot_general | solution.py:47
  82.2 0.4 fusion.55
  82.6 1.3 %fusion.56 = f32[8,256,64]{1,2,0:T(8,128)S(1)} fusion(f32[8,256,64]{1,2,0:T(8,128)S(1)} %get-tuple-element.220, s32[]{:T(128)S(6)} %copy.62, pred[256,640]{1,0:T(32,128)(4,1)S(1)} %fusion.53, f32[256,640]{1,0:T(8,128)S(1)} %get-tuple-element.203, f32[256]{0:T(256)S(1)} %broadcast_maximum_fusion.2, bf16[8,640,64]{2,1,0:T(8,128)(2,1)} %get-tuple-element.235, ...), kind=kOutput, calls=%fused_computation.7.clone.1 | convolution fusion | flops 21479424 | bytes 1051648 | tf_op jit(solution)/shard_map/while/body/eval_jaxpr/dot_general | solution.py:55
  84.1 1.3 %fusion.54 = (f32[256]{0:T(256)S(1)}, f32[256,640]{1,0:T(8,128)S(1)}) fusion(pred[256,640]{1,0:T(32,128)(4,1)S(1)} %fusion.53, bf16[8,640,64]{2,1,0:T(8,128)(2,1)} %get-tuple-element.234, s32[]{:T(128)S(6)} %copy.62, bf16[8,256,64]{1,2,0:T(8,128)(2,1)} %get-tuple-element.233), kind=kOutput, calls=%fused_computation.76.clone.1 | convolution fusion | flops 21462784 | bytes 1017856 | tf_op jit(solution)/shard_map/while/body/eval_jaxpr/qd,kd->qk/dot_general | solution.py:47
  85.8 1.3 %fusion.56 = f32[8,256,64]{1,2,0:T(8,128)S(1)} fusion(f32[8,256,64]{1,2,0:T(8,128)S(1)} %get-tuple-element.220, s32[]{:T(128)S(6)} %copy.62, pred[256,640]{1,0:T(32,128)(4,1)S(1)} %fusion.53, f32[256,640]{1,0:T(8,128)S(1)} %get-tuple-element.203, f32[256]{0:T(256)S(1)} %broadcast_maximum_fusion.2, bf16[8,640,64]{2,1,0:T(8,128)(2,1)} %get-tuple-element.235, ...), kind=kOutput, calls=%fused_computation.7.clone.1 | convolution fusion | flops 21479424 | bytes 1051648 | tf_op jit(solution)/shard_map/while/body/eval_jaxpr/dot_general | solution.py:55
  87.2 2.2 %all_gather.7 = bf16[256,1024]{0,1:T(8,128)(2,1)S(1)} all-gather(bf16[256,512]{0,1:T(8,128)(2,1)S(1)} %bitcast.72), channel_id=1, replica_groups=mesh['dp'=4,'kv'=4,'tp'=2] {'tp'}, dimensions={1}, use_global_device_ids=true | all-gather | bytes 786432 | tf_op jit(solution)/shard_map/all_gather | solution.py:139
  89.3 1.5 %convolution_convert_fusion = bf16[256,1024]{1,0:T(8,128)(2,1)} fusion(bf16[256,1024]{0,1:T(8,128)(2,1)S(1)} %all_gather.7, bf16[1024,1024]{1,0:T(8,128)(2,1)S(1)} %copy-done), kind=kOutput, calls=%fused_computation.29 | convolution fusion | flops 537133056 | bytes 3145728 | tf_op jit(solution)/shard_map/dot_general | solution.py:138
  (88 shorter events, 5.6 us)
Async XLA Ops:
  6.5 82.8 %copy-start = (bf16[1024,1024]{1,0:T(8,128)(2,1)S(1)}, bf16[1024,1024]{1,0:T(8,128)(2,1)}, u32[]{:S(2)}) copy-start(bf16[1024,1024]{1,0:T(8,128)(2,1)} %param.12) | copy-start | bytes 6291460
  6.5 14.9 %all-gather.2.cloned.1.call-start = ((), (), s32[]{:S(2)}) async-start(), calls=%async_computation.3 | async-start | bytes 1572864 | tf_op jit(solution)/shard_map/all_gather | solution.py:72
  9.3 11.8 %all-to-all-start = ((s32[4,1,3]{2,1,0:T(1,128)}), s32[4,1,3]{2,1,0:T(1,128)S(1)}, u32[]{:S(2)}, u32[]{:S(2)}) async-start(s32[4,1,3]{2,1,0:T(1,128)} %copy.41), calls=%async_computation | async-start | bytes 4096 | tf_op jit(solution)/shard_map/all_to_all | solution.py:105
  16.0 8.4 %copy-start.4 = (f32[256,32]{0,1:T(8,128)}, f32[256,32]{0,1:T(8,128)S(1)}, u32[]{:S(2)}) copy-start(f32[256,32]{0,1:T(8,128)S(1)} %get-tuple-element.133) | copy-start | bytes 98308
  16.0 8.4 %copy-start.5 = (f32[256,32]{0,1:T(8,128)}, f32[256,32]{0,1:T(8,128)S(1)}, u32[]{:S(2)}) copy-start(f32[256,32]{0,1:T(8,128)S(1)} %get-tuple-element.134) | copy-start | bytes 98308
  24.3 7.4 %copy-start.7 = (s32[8,16]{1,0:T(8,128)S(1)}, s32[8,16]{1,0:T(8,128)}, u32[]{:S(2)}) copy-start(s32[8,16]{1,0:T(8,128)} %param.13) | copy-start | bytes 1540
  26.4 16.2 %all-to-all-start.1 = ((bf16[4,3,32,512]{3,2,1,0:T(8,128)(2,1)}), bf16[4,3,32,512]{3,2,1,0:T(8,128)(2,1)S(1)}, u32[]{:S(2)}, u32[]{:S(2)}) async-start(bf16[4,3,32,512]{3,2,1,0:T(8,128)(2,1)} %bitcast.5), calls=%async_computation.1 | async-start | bytes 786432 | tf_op jit(solution)/shard_map/all_to_all | solution.py:109
  42.7 7.8 %copy-start.2 = (bf16[4,3,32,512]{3,2,1,0:T(8,128)(2,1)}, bf16[4,3,32,512]{3,2,1,0:T(8,128)(2,1)S(1)}, u32[]{:S(2)}) copy-start(bf16[4,3,32,512]{3,2,1,0:T(8,128)(2,1)S(1)} %all-to-all-done.1) | copy-start | bytes 1179652
  42.7 15.5 %all-to-all-start.2 = ((bf16[4,3,32,512]{3,2,1,0:T(8,128)(2,1)}), bf16[4,3,32,512]{3,2,1,0:T(8,128)(2,1)}, u32[]{:S(2)}, u32[]{:S(2)}) async-start(bf16[4,3,32,512]{3,2,1,0:T(8,128)(2,1)} %bitcast.9), calls=%async_computation.2 | async-start | bytes 786432 | tf_op jit(solution)/shard_map/all_to_all | solution.py:110
  55.3 4.4 %copy-start.1 = (bf16[256,8,64]{2,1,0:T(8,128)(2,1)S(1)}, bf16[256,8,64]{2,1,0:T(8,128)(2,1)}, u32[]{:S(2)}) copy-start(bf16[256,8,64]{2,1,0:T(8,128)(2,1)} %copy.46) | copy-start | bytes 786436
  59.7 1.6 %copy-start.6 = (pred[640]{0:T(1024)(128)(4,1)S(1)}, pred[640]{0:T(1024)(128)(4,1)}, u32[]{:S(2)}) copy-start(pred[640]{0:T(1024)(128)(4,1)} %concatenate.45) | copy-start | bytes 1924
  59.7 1.6 %copy-start.8 = (f32[8,256]{1,0:T(8,128)S(1)}, f32[8,256]{1,0:T(8,128)}, u32[]{:S(2)}) copy-start(f32[8,256]{1,0:T(8,128)} %custom-call.4) | copy-start | bytes 24580
  60.0 1.3 %copy-start.3 = (f32[8,256,64]{1,2,0:T(8,128)S(1)}, f32[8,256,64]{1,2,0:T(8,128)}, u32[]{:S(2)}) copy-start(f32[8,256,64]{1,2,0:T(8,128)} %custom-call.5) | copy-start | bytes 1572868
Sparse Core Ops, SparseCore 0:
  8.9 11.7 all-gather.1
where the time goes:
time: 98.5 us; the launch traced here: 97.7 us
  matrix products  31.3 us (32%)
  starting transfers between devices  14.6 us (15%)
  waiting for transfers between devices  14.3 us (15%)
  between operations  13.7 us (14%)
  local copies, waits for them, and re-layouts  13.3 us (14%)
  other arithmetic  8.01 us (8%)
  blocking collectives  2.18 us (2%)
    dot_general x8, matrix products, one_head(): jnp.einsum('qd,kd->qk', query_head, key_head, preferred_element_type=jnp....  10.5 us
    dot_general x8, matrix products, one_head(): jnp.dot(weights.astype(jnp.bfloat16), value_head, preferred_element_type=...  10.2 us
    dot_general x3, matrix products, on_device(): jnp.dot(fragment, weight, preferred_element_type=jnp.float32)  9.11 us
    all_to_all x1, waiting for transfers between devices, on_device(): lax.all_to_all(key_store[incoming], 'kv', split_axis=0, concat_axis=0, ti...  6.89 us
    all_to_all x1, starting transfers between devices, on_device(): lax.all_to_all(request, 'kv', split_axis=0, concat_axis=0, tiled=True)  6.35 us
    all_to_all x1, waiting for transfers between devices, on_device(): lax.all_to_all(request, 'kv', split_axis=0, concat_axis=0, tiled=True)  5.08 us
    all_to_all x1, starting transfers between devices, on_device(): lax.all_to_all(value_store[incoming], 'kv', split_axis=0, concat_axis=0,...  4.12 us
    all_to_all x1, starting transfers between devices, on_device(): lax.all_to_all(key_store[incoming], 'kv', split_axis=0, concat_axis=0, ti...  4.09 us
  transfers between devices with their start and end apart: 4, of which 3 were waited for; matrix products, arithmetic and copies ran while one was open for 18% of the time, Pallas kernels for 0%

commit v1 on v0

v1 whole, which is shorter than its diff:
```python
import functools

import jax
import jax.numpy as jnp
import numpy as np
from jax import lax
from jax.experimental import pallas as pl
from jax.experimental.pallas import tpu as pltpu
from jax.sharding import PartitionSpec as P

HEAD_DIM = 64
BLOCK = 32
CAP = 3
LANES = 128
ROTARY_BASE = 500000.0
MASKED = -1e30
MESH = pl.DeviceIdType.MESH
F32 = jnp.float32
BF16 = jnp.bfloat16


def rotary_tables(rows, devices):
    half = HEAD_DIM // 2
    inverse = (1.0 / ROTARY_BASE ** (np.arange(half, dtype=np.float64) / half))
    lanes = np.tile(inverse, LANES // half)[None, :]
    row_angle = np.arange(rows, dtype=np.float64)[:, None] * lanes
    base_angle = (np.arange(devices, dtype=np.float64) * rows)[:, None] * lanes
    pack = lambda a: np.concatenate([np.cos(a), np.sin(a)], axis=1).astype(np.float32)
    return pack(row_angle), pack(base_angle)


def listed_columns(chosen, holder, rows):
    blocks = rows // BLOCK
    ids = holder * blocks + lax.broadcasted_iota(jnp.int32, (blocks, rows), 1) // BLOCK
    hit = jnp.zeros((blocks, rows), F32)
    for slot in range(chosen.shape[1]):
        hit = jnp.where(chosen[:, slot : slot + 1] == ids, 1.0, hit)
    return hit


def selection(hit, earlier):
    blocks, rows = hit.shape
    need = jnp.broadcast_to(jnp.max(hit, axis=0, keepdims=True), hit.shape)
    rank = jnp.dot(need.astype(BF16), earlier, preferred_element_type=F32)
    shape = (CAP * BLOCK, rows)
    slot_row = lax.broadcasted_iota(jnp.int32, shape, 0)
    column = lax.broadcasted_iota(jnp.int32, shape, 1)
    wanted = (slot_row // BLOCK).astype(F32)
    place = jnp.where(need[:1] > 0.5, rank[:1], -1.0)
    same = (slot_row % BLOCK) == (column % BLOCK)
    return jnp.where(same & (place == wanted), 1.0, 0.0).astype(BF16)


def layer(
    devices,
    chosen_ref, base_ref, row_hbm, tok_hbm, wq_hbm, wk_hbm, wv_hbm, wo_hbm,
    out_ref,
    tab, tok_own, tok_peer, wq, wk, wv, wo, q_acc, k_acc, v_acc, k_own, v_own, q2,
    lists, k_send, v_send, k_recv, v_recv, peak, total, summed, att_own, att_peer,
    load_sem, tok_sem, att_sem, list_send, list_recv, key_send, key_recv,
):
    me = lax.axis_index("kv")
    core = lax.axis_index("tp")
    rows, half = tok_own.shape
    head_width = k_own.shape[1]
    pairs = head_width // LANES
    picked = CAP * BLOCK
    other = 1 - core

    loads = [
        pltpu.make_async_copy(src, dst, load_sem.at[i])
        for i, (src, dst) in enumerate(
            ((tok_hbm, tok_own), (wk_hbm, wk), (row_hbm, tab), (wv_hbm, wv), (wq_hbm, wq), (wo_hbm, wo))
        )
    ]
    for load in loads:
        load.start()
    tok_load, wk_load, tab_load, wv_load, wq_load, wo_load = loads

    barrier = pltpu.get_barrier_semaphore()
    pl.semaphore_signal(barrier, inc=1, device_id={"tp": other}, device_id_type=MESH)

    def greet(d, _):
        pl.semaphore_signal(
            barrier, inc=1, device_id={"kv": lax.rem(me + d, devices)}, device_id_type=MESH
        )
        return 0

    lax.fori_loop(1, devices, greet, 0)

    own_half = pl.ds(pl.multiple_of(core * half, half), half)
    peer_half = pl.ds(pl.multiple_of(other * half, half), half)

    tok_load.wait()
    wk_load.wait()
    k_acc[...] = jnp.dot(tok_own[...], wk[own_half, :], preferred_element_type=F32)

    pl.semaphore_wait(barrier, devices)
    tok_copy = pltpu.make_async_remote_copy(
        src_ref=tok_own, dst_ref=tok_peer, send_sem=tok_sem.at[0], recv_sem=tok_sem.at[1],
        device_id={"tp": other}, device_id_type=MESH,
    )
    tok_copy.start()

    def list_copy(d, target):
        return pltpu.make_async_remote_copy(
            src_ref=chosen_ref, dst_ref=lists.at[d], send_sem=list_send.at[d],
            recv_sem=list_recv.at[d], device_id={"kv": target}, device_id_type=MESH,
        )

    def send_list(d, _):
        list_copy(d, me - d).start()
        return 0

    lax.fori_loop(1, me + 1, send_list, 0)

    wv_load.wait()
    v_acc[...] = jnp.dot(tok_own[...], wv[own_half, :], preferred_element_type=F32)
    wq_load.wait()
    q_acc[...] = jnp.dot(tok_own[...], wq[own_half, :], preferred_element_type=F32)

    tab_load.wait()
    lane = lax.broadcasted_iota(jnp.int32, (rows, LANES), 1)
    first = (lane % HEAD_DIM) < HEAD_DIM // 2
    base = base_ref[pl.ds(me, 1), :]
    row_cos, row_sin = tab[:, :LANES], tab[:, LANES:]
    base_cos, base_sin = base[:, :LANES], base[:, LANES:]
    cosine = row_cos * base_cos - row_sin * base_sin
    sine = row_sin * base_cos + row_cos * base_sin
    sine = jnp.where(first, -sine, sine)
    tab[:, :LANES] = cosine
    tab[:, LANES:] = sine

    def rotated(x):
        swapped = jnp.where(
            first,
            pltpu.roll(x, LANES - HEAD_DIM // 2, axis=1),
            pltpu.roll(x, HEAD_DIM // 2, axis=1),
        )
        return x * tab[:, :LANES] + swapped * tab[:, LANES:]

    row_i = lax.broadcasted_iota(jnp.int32, (rows, rows), 0)
    col_i = lax.broadcasted_iota(jnp.int32, (rows, rows), 1)
    earlier = jnp.where((row_i % BLOCK == 0) & (row_i // BLOCK < col_i // BLOCK), 1.0, 0.0).astype(BF16)

    tok_copy.wait_recv()
    k_full = k_acc[...] + jnp.dot(tok_peer[...], wk[peer_half, :], preferred_element_type=F32)
    for i in range(pairs):
        tile = slice(i * LANES, (i + 1) * LANES)
        k_own[:, tile] = rotated(k_full[:, tile]).astype(BF16)

    def row_copy(kind, d, target):
        source, landing = ((k_send, k_recv), (v_send, v_recv))[kind]
        return pltpu.make_async_remote_copy(
            src_ref=source.at[d], dst_ref=landing.at[d], send_sem=key_send.at[kind, d],
            recv_sem=key_recv.at[kind, d], device_id={"kv": target}, device_id_type=MESH,
        )

    def send_keys(step, _):
        d = devices - 1 - me - step
        list_copy(d, me).wait_recv()
        pick = selection(listed_columns(lists[d], me, rows), earlier)
        k_send[d] = jnp.dot(pick, k_own[...], preferred_element_type=F32).astype(BF16)
        row_copy(0, d, me + d).start()
        return 0

    lax.fori_loop(0, devices - 1 - me, send_keys, 0)

    v_own[...] = (
        v_acc[...] + jnp.dot(tok_peer[...], wv[peer_half, :], preferred_element_type=F32)
    ).astype(BF16)

    def send_values(step, _):
        d = devices - 1 - me - step
        pick = selection(listed_columns(lists[d], me, rows), earlier)
        v_send[d] = jnp.dot(pick, v_own[...], preferred_element_type=F32).astype(BF16)
        row_copy(1, d, me + d).start()
        return 0

    lax.fori_loop(0, devices - 1 - me, send_values, 0)

    q_full = q_acc[...] + jnp.dot(tok_peer[...], wq[peer_half, :], preferred_element_type=F32)
    for i in range(pairs):
        tile = slice(i * LANES, (i + 1) * LANES)
        q = rotated(q_full[:, tile]).astype(BF16).astype(F32) * (HEAD_DIM**-0.5)
        q2[i, :rows, :] = jnp.where(lane < HEAD_DIM, q, 0.0).astype(BF16)
        q2[i, rows:, :] = jnp.where(lane < HEAD_DIM, 0.0, q).astype(BF16)

    chosen = chosen_ref[...]

    def spread(hit):
        keys = hit.shape[1]
        blocks = hit.shape[0]
        wide = jnp.broadcast_to(hit[:, None, :], (blocks, BLOCK, keys))
        return wide.reshape(blocks * BLOCK, keys)

    def scores_of(i, keys):
        return lax.dot_general(
            q2[i], keys, (((1,), (1,)), ((), ())), preferred_element_type=F32
        )

    listed = spread(listed_columns(chosen, me, rows))
    bias = jnp.where((listed > 0.5) & (col_i <= row_i), 0.0, MASKED)
    bias = jnp.concatenate([bias, bias], axis=0)
    for i in range(pairs):
        tile = slice(i * LANES, (i + 1) * LANES)
        scores = scores_of(i, k_own[:, tile]) + bias
        top = jnp.max(scores, axis=1, keepdims=True)
        weights = jnp.exp(scores - top)
        peak[i] = top
        total[i] = jnp.sum(weights, axis=1, keepdims=True)
        summed[i] = jnp.dot(weights.astype(BF16), v_own[:, tile], preferred_element_type=F32)

    def attend(d, _):
        hit = listed_columns(chosen, me - d, rows)
        pick = selection(hit, earlier)
        got = lax.dot_general(
            hit.astype(BF16), pick, (((1,), (1,)), ((), ())), preferred_element_type=F32
        )
        far = jnp.where(spread(got) > 0.5, 0.0, MASKED)
        far = jnp.concatenate([far, far], axis=0)
        row_copy(0, d, me).wait_recv()
        row_copy(1, d, me).wait_recv()
        for i in range(pairs):
            tile = slice(i * LANES, (i + 1) * LANES)
            scores = scores_of(i, k_recv[d, :, tile]) + far
            old = peak[i]
            top = jnp.maximum(old, jnp.max(scores, axis=1, keepdims=True))
            factor = jnp.exp(old - top)
            weights = jnp.exp(scores - top)
            peak[i] = top
            total[i] = total[i] * factor + jnp.sum(weights, axis=1, keepdims=True)
            summed[i] = summed[i] * factor + jnp.dot(
                weights.astype(BF16), v_recv[d, :, tile], preferred_element_type=F32
            )
        return 0

    lax.fori_loop(1, me + 1, attend, 0)

    for i in range(pairs):
        tile = slice(i * LANES, (i + 1) * LANES)
        ratio = summed[i] / total[i]
        att_own[:, tile] = jnp.where(lane < HEAD_DIM, ratio[:rows], ratio[rows:]).astype(BF16)
    att_copy = pltpu.make_async_remote_copy(
        src_ref=att_own, dst_ref=att_peer, send_sem=att_sem.at[0], recv_sem=att_sem.at[1],
        device_id={"tp": other}, device_id_type=MESH,
    )
    att_copy.start()
    wo_load.wait()
    own_rows = pl.ds(pl.multiple_of(core * head_width, head_width), head_width)
    peer_rows = pl.ds(pl.multiple_of(other * head_width, head_width), head_width)
    mixed = jnp.dot(att_own[...], wo[own_rows, :], preferred_element_type=F32)
    att_copy.wait_recv()
    mixed = mixed + jnp.dot(att_peer[...], wo[peer_rows, :], preferred_element_type=F32)
    out_ref[...] = mixed.astype(BF16)

    att_copy.wait_send()
    tok_copy.wait_send()

    def drain_list(d, _):
        list_copy(d, me - d).wait_send()
        return 0

    lax.fori_loop(1, me + 1, drain_list, 0)

    def drain_rows(d, _):
        row_copy(0, d, me + d).wait_send()
        row_copy(1, d, me + d).wait_send()
        return 0

    lax.fori_loop(1, devices - me, drain_rows, 0)


def on_device(devices, tokens, query_weight, key_weight, value_weight, out_weight, chosen):
    rows, half = tokens.shape
    width, head_width = query_weight.shape
    pairs = head_width // LANES
    picked = CAP * BLOCK
    row_table, base_table = rotary_tables(rows, devices)
    vmem = pl.BlockSpec(memory_space=pltpu.VMEM)
    anywhere = pl.BlockSpec(memory_space=pl.ANY)
    dma = pltpu.SemaphoreType.DMA
    return pl.pallas_call(
        functools.partial(layer, devices),
        out_shape=jax.ShapeDtypeStruct((rows, out_weight.shape[1]), BF16),
        in_specs=[vmem, vmem] + [anywhere] * 6,
        out_specs=vmem,
        scratch_shapes=[
            pltpu.VMEM((rows, 2 * LANES), F32),
            pltpu.VMEM((rows, half), BF16),
            pltpu.VMEM((rows, half), BF16),
            pltpu.VMEM((width, head_width), BF16),
            pltpu.VMEM((width, head_width), BF16),
            pltpu.VMEM((width, head_width), BF16),
            pltpu.VMEM(out_weight.shape, BF16),
            pltpu.VMEM((rows, head_width), F32),
            pltpu.VMEM((rows, head_width), F32),
            pltpu.VMEM((rows, head_width), F32),
            pltpu.VMEM((rows, head_width), BF16),
            pltpu.VMEM((rows, head_width), BF16),
            pltpu.VMEM((pairs, 2 * rows, LANES), BF16),
            pltpu.VMEM((devices,) + chosen.shape, jnp.int32),
            pltpu.VMEM((devices, picked, head_width), BF16),
            pltpu.VMEM((devices, picked, head_width), BF16),
            pltpu.VMEM((devices, picked, head_width), BF16),
            pltpu.VMEM((devices, picked, head_width), BF16),
            pltpu.VMEM((pairs, 2 * rows, 1), F32),
            pltpu.VMEM((pairs, 2 * rows, 1), F32),
            pltpu.VMEM((pairs, 2 * rows, LANES), F32),
            pltpu.VMEM((rows, head_width), BF16),
            pltpu.VMEM((rows, head_width), BF16),
            dma((6,)),
            dma((2,)),
            dma((2,)),
            dma((devices,)),
            dma((devices,)),
            dma((2, devices)),
            dma((2, devices)),
        ],
        compiler_params=pltpu.CompilerParams(
            collective_id=0, has_side_effects=True, vmem_limit_bytes=60 * 1024 * 1024
        ),
        name="layer",
    )(
        chosen, jnp.asarray(base_table), jnp.asarray(row_table), tokens,
        query_weight, key_weight, value_weight, out_weight,
    )


def solution(mesh):
    placed = (
        P(("dp", "kv"), "tp"),
        P(None, "tp"),
        P(None, "tp"),
        P(None, "tp"),
        P(None, "tp"),
        P(("dp", "kv"), None),
    )
    return jax.shard_map(
        functools.partial(on_device, mesh.shape["kv"]),
        mesh=mesh, in_specs=placed, out_specs=P(("dp", "kv"), "tp"), check_vma=False,
    )
```

time: 98.5 us -> 35.2 us (0.36)
  the two profiles are of different devices: /device:TPU:0 before, /device:TPU:17 now
where the time goes in v1:
time: 35.2 us; the launch traced here: 35 us
  Pallas kernels  33.1 us (94%)
  local copies, waits for them, and re-layouts  1.87 us (5%)
    pallas_call x1, Pallas kernels, on_device(): pl.pallas_call(functools.partial(layer, devices), out_shape=jax.ShapeDtyp...  33.1 us
    unnamed x1, local copies, waits for them, and re-layouts  1.87 us

profile of v1, /device:TPU:17, one launch (start us, length us, event | category | flops | bytes accessed | tf_op | source)
XLA Modules:
  0.0 35.0 jit_solution(10795732500307669581)
XLA Ops:
  0.0 33.1 %layer.1 = bf16[256,1024]{1,0:T(8,128)(2,1)} custom-call(s32[8,16]{1,0:T(8,128)} %chosen_ref.1, f32[4,256]{1,0:T(4,128)} %constant.4.clone.base_ref, f32[256,256]{1,0:T(8,128)} %constant.5.clone.row_hbm, bf16[256,1024]{1,0:T(8,128)(2,1)} %tok_hbm.1, bf16[2048,512]{1,0:T(8,128)(2,1)} %wq_hbm.1, bf16[2048,512]{1,0:T(8,128)(2,1)} %wk_hbm.1, ...), custom_call_target="tpu_custom_call" | custom-call | tf_op jit(solution)/shard_map/layer/pallas_call | solution.py:283
  33.1 1.9 %copy.10 = bf16[256,1024]{1,0:T(8,128)(2,1)} copy(bf16[256,1024]{1,0:T(8,128)(2,1)} %layer.1) | data formatting | bytes 1048576

commit v2 on v1

--- a/solution.py
+++ b/solution.py
@@ -53,11 +53,11 @@
 
 def layer(
     devices,
-    chosen_ref, base_ref, row_hbm, tok_hbm, wq_hbm, wk_hbm, wv_hbm, wo_hbm,
+    chosen_hbm, base_hbm, row_hbm, tok_hbm, wq_hbm, wk_hbm, wv_hbm, wo_hbm,
     out_ref,
-    tab, tok_own, tok_peer, wq, wk, wv, wo, q_acc, k_acc, v_acc, k_own, v_own, q2,
-    lists, k_send, v_send, k_recv, v_recv, peak, total, summed, att_own, att_peer,
-    load_sem, tok_sem, att_sem, list_send, list_recv, key_send, key_recv,
+    chosen_ref, base_ref, tab, tok_own, tok_peer, wq, wk, wv, wo, q_acc, k_acc, v_acc, k_own, v_own, q2,
+    lists, picks, k_send, v_send, k_recv, v_recv, peak, total, summed, weigh, att_own, att_peer,
+    load_sem, tok_sem, att_sem, list_send, list_recv, key_send, key_recv, root_send, root_recv,
 ):
     me = lax.axis_index("kv")
     core = lax.axis_index("tp")
@@ -70,12 +70,12 @@
     loads = [
         pltpu.make_async_copy(src, dst, load_sem.at[i])
         for i, (src, dst) in enumerate(
-            ((tok_hbm, tok_own), (wk_hbm, wk), (row_hbm, tab), (wv_hbm, wv), (wq_hbm, wq), (wo_hbm, wo))
+            ((chosen_hbm, chosen_ref), (base_hbm, base_ref), (tok_hbm, tok_own), (wk_hbm, wk), (row_hbm, tab), (wv_hbm, wv), (wq_hbm, wq), (wo_hbm, wo))
         )
     ]
     for load in loads:
         load.start()
-    tok_load, wk_load, tab_load, wv_load, wq_load, wo_load = loads
+    chosen_load, base_load, tok_load, wk_load, tab_load, wv_load, wq_load, wo_load = loads
 
     barrier = pltpu.get_barrier_semaphore()
     pl.semaphore_signal(barrier, inc=1, device_id={"tp": other}, device_id_type=MESH)
@@ -96,30 +96,32 @@
     k_acc[...] = jnp.dot(tok_own[...], wk[own_half, :], preferred_element_type=F32)
 
     pl.semaphore_wait(barrier, devices)
+
+    def list_copy(d, target):
+        return pltpu.make_async_remote_copy(
+            src_ref=chosen_ref, dst_ref=lists.at[d], send_sem=list_send.at[d],
+            recv_sem=list_recv.at[d], device_id={"kv": target}, device_id_type=MESH,
+        )
+
+    def send_list(d, _):
+        list_copy(d, me - d).start()
+        return 0
+
+    chosen_load.wait()
+    lax.fori_loop(1, me + 1, send_list, 0)
     tok_copy = pltpu.make_async_remote_copy(
         src_ref=tok_own, dst_ref=tok_peer, send_sem=tok_sem.at[0], recv_sem=tok_sem.at[1],
         device_id={"tp": other}, device_id_type=MESH,
     )
     tok_copy.start()
 
-    def list_copy(d, target):
-        return pltpu.make_async_remote_copy(
-            src_ref=chosen_ref, dst_ref=lists.at[d], send_sem=list_send.at[d],
-            recv_sem=list_recv.at[d], device_id={"kv": target}, device_id_type=MESH,
-        )
-
-    def send_list(d, _):
-        list_copy(d, me - d).start()
-        return 0
-
-    lax.fori_loop(1, me + 1, send_list, 0)
-
     wv_load.wait()
     v_acc[...] = jnp.dot(tok_own[...], wv[own_half, :], preferred_element_type=F32)
     wq_load.wait()
     q_acc[...] = jnp.dot(tok_own[...], wq[own_half, :], preferred_element_type=F32)
 
     tab_load.wait()
+    base_load.wait()
     lane = lax.broadcasted_iota(jnp.int32, (rows, LANES), 1)
     first = (lane % HEAD_DIM) < HEAD_DIM // 2
     base = base_ref[pl.ds(me, 1), :]
@@ -149,32 +151,70 @@
         tile = slice(i * LANES, (i + 1) * LANES)
         k_own[:, tile] = rotated(k_full[:, tile]).astype(BF16)
 
-    def row_copy(kind, d, target):
-        source, landing = ((k_send, k_recv), (v_send, v_recv))[kind]
+    buffers = ((k_own, k_send, k_recv), (v_own, v_send, v_recv))
+
+    def row_copy(kind, d, target, holder):
+        _, source, landing = buffers[kind]
+
+        def part(span):
+            return pltpu.make_async_remote_copy(
+                src_ref=source.at[d, span], dst_ref=landing.at[d, span],
+                send_sem=key_send.at[kind, d], recv_sem=key_recv.at[kind, d],
+                device_id={"kv": target}, device_id_type=MESH,
+            )
+
+        return part(slice(BLOCK, picked)), part(slice(0, picked)), holder == 0
+
+    def each(copies, act):
+        short, whole, is_short = copies
+        pl.when(is_short)(lambda: act(short))
+        pl.when(jnp.logical_not(is_short))(lambda: act(whole))
+
+    def root_copy(kind, from_own):
+        own, _, landing = buffers[kind]
+        block = slice(0, BLOCK)
+        source = own.at[block] if from_own else landing.at[me, block]
         return pltpu.make_async_remote_copy(
-            src_ref=source.at[d], dst_ref=landing.at[d], send_sem=key_send.at[kind, d],
-            recv_sem=key_recv.at[kind, d], device_id={"kv": target}, device_id_type=MESH,
-        )
-
-    def send_keys(step, _):
-        d = devices - 1 - me - step
+            src_ref=source, dst_ref=landing.at[lax.rem(me + 1, devices), block],
+            send_sem=root_send.at[kind], recv_sem=root_recv.at[kind],
+            device_id={"kv": lax.rem(me + 1, devices)}, device_id_type=MESH,
+        )
+
+    def root_arrival(kind):
+        landing = buffers[kind][2]
+        block = slice(0, BLOCK)
+        return pltpu.make_async_remote_copy(
+            src_ref=landing.at[me, block], dst_ref=landing.at[me, block],
+            send_sem=root_send.at[kind], recv_sem=root_recv.at[kind],
+            device_id={"kv": lax.rem(me + 1, devices)}, device_id_type=MESH,
+        )
+
+    @pl.when(me == 0)
+    def _():
+        root_copy(0, True).start()
+
+    def send_keys(d, _):
         list_copy(d, me).wait_recv()
         pick = selection(listed_columns(lists[d], me, rows), earlier)
+        picks[d] = pick
         k_send[d] = jnp.dot(pick, k_own[...], preferred_element_type=F32).astype(BF16)
-        row_copy(0, d, me + d).start()
-        return 0
-
-    lax.fori_loop(0, devices - 1 - me, send_keys, 0)
+        each(row_copy(0, d, me + d, me), lambda c: c.start())
+        return 0
+
+    lax.fori_loop(1, devices - me, send_keys, 0)
 
     v_own[...] = (
         v_acc[...] + jnp.dot(tok_peer[...], wv[peer_half, :], preferred_element_type=F32)
     ).astype(BF16)
 
+    @pl.when(me == 0)
+    def _():
+        root_copy(1, True).start()
+
     def send_values(step, _):
         d = devices - 1 - me - step
-        pick = selection(listed_columns(lists[d], me, rows), earlier)
-        v_send[d] = jnp.dot(pick, v_own[...], preferred_element_type=F32).astype(BF16)
-        row_copy(1, d, me + d).start()
+        v_send[d] = jnp.dot(picks[d], v_own[...], preferred_element_type=F32).astype(BF16)
+        each(row_copy(1, d, me + d, me), lambda c: c.start())
         return 0
 
     lax.fori_loop(0, devices - 1 - me, send_values, 0)
@@ -199,6 +239,16 @@
             q2[i], keys, (((1,), (1,)), ((), ())), preferred_element_type=F32
         )
 
+    def relay(kind):
+        @pl.when(me > 0)
+        def _():
+            root_arrival(kind).wait_recv()
+
+            @pl.when(me < devices - 1)
+            def _():
+                root_copy(kind, False).start()
+
+    relay(0)
     listed = spread(listed_columns(chosen, me, rows))
     bias = jnp.where((listed > 0.5) & (col_i <= row_i), 0.0, MASKED)
     bias = jnp.concatenate([bias, bias], axis=0)
@@ -210,8 +260,10 @@
         peak[i] = top
         total[i] = jnp.sum(weights, axis=1, keepdims=True)
         summed[i] = jnp.dot(weights.astype(BF16), v_own[:, tile], preferred_element_type=F32)
-
-    def attend(d, _):
+    relay(1)
+
+    def attend(step, _):
+        d = jnp.where(me == devices - 1, step, me + 1 - step)
         hit = listed_columns(chosen, me - d, rows)
         pick = selection(hit, earlier)
         got = lax.dot_general(
@@ -219,8 +271,7 @@
         )
         far = jnp.where(spread(got) > 0.5, 0.0, MASKED)
         far = jnp.concatenate([far, far], axis=0)
-        row_copy(0, d, me).wait_recv()
-        row_copy(1, d, me).wait_recv()
+        each(row_copy(0, d, me, me - d), lambda c: c.wait_recv())
         for i in range(pairs):
             tile = slice(i * LANES, (i + 1) * LANES)
             scores = scores_of(i, k_recv[d, :, tile]) + far
@@ -230,31 +281,39 @@
             weights = jnp.exp(scores - top)
             peak[i] = top
             total[i] = total[i] * factor + jnp.sum(weights, axis=1, keepdims=True)
-            summed[i] = summed[i] * factor + jnp.dot(
-                weights.astype(BF16), v_recv[d, :, tile], preferred_element_type=F32
+            summed[i] = summed[i] * factor
+            weigh[i] = weights.astype(BF16)
+        each(row_copy(1, d, me, me - d), lambda c: c.wait_recv())
+        for i in range(pairs):
+            tile = slice(i * LANES, (i + 1) * LANES)
+            summed[i] += jnp.dot(weigh[i], v_recv[d, :, tile], preferred_element_type=F32)
+        return 0
+
+    lax.fori_loop(1, me + 1, attend, 0)
+
+    att_copies = []
+    for i in range(pairs):
+        ratio = summed[i] / total[i]
+        att_own[i] = jnp.where(lane < HEAD_DIM, ratio[:rows], ratio[rows:]).astype(BF16)
+        att_copies.append(
+            pltpu.make_async_remote_copy(
+                src_ref=att_own.at[i], dst_ref=att_peer.at[i], send_sem=att_sem.at[0, i],
+                recv_sem=att_sem.at[1, i], device_id={"tp": other}, device_id_type=MESH,
             )
-        return 0
-
-    lax.fori_loop(1, me + 1, attend, 0)
-
-    for i in range(pairs):
-        tile = slice(i * LANES, (i + 1) * LANES)
-        ratio = summed[i] / total[i]
-        att_own[:, tile] = jnp.where(lane < HEAD_DIM, ratio[:rows], ratio[rows:]).astype(BF16)
-    att_copy = pltpu.make_async_remote_copy(
-        src_ref=att_own, dst_ref=att_peer, send_sem=att_sem.at[0], recv_sem=att_sem.at[1],
-        device_id={"tp": other}, device_id_type=MESH,
-    )
-    att_copy.start()
+        )
+        att_copies[-1].start()
     wo_load.wait()
     own_rows = pl.ds(pl.multiple_of(core * head_width, head_width), head_width)
     peer_rows = pl.ds(pl.multiple_of(other * head_width, head_width), head_width)
-    mixed = jnp.dot(att_own[...], wo[own_rows, :], preferred_element_type=F32)
-    att_copy.wait_recv()
-    mixed = mixed + jnp.dot(att_peer[...], wo[peer_rows, :], preferred_element_type=F32)
+    joined = lambda ref: jnp.concatenate([ref[i] for i in range(pairs)], axis=1)
+    mixed = jnp.dot(joined(att_own), wo[own_rows, :], preferred_element_type=F32)
+    for copy in att_copies:
+        copy.wait_recv()
+    mixed = mixed + jnp.dot(joined(att_peer), wo[peer_rows, :], preferred_element_type=F32)
     out_ref[...] = mixed.astype(BF16)
 
-    att_copy.wait_send()
+    for copy in att_copies:
+        copy.wait_send()
     tok_copy.wait_send()
 
     def drain_list(d, _):
@@ -264,11 +323,16 @@
     lax.fori_loop(1, me + 1, drain_list, 0)
 
     def drain_rows(d, _):
-        row_copy(0, d, me + d).wait_send()
-        row_copy(1, d, me + d).wait_send()
+        each(row_copy(0, d, me + d, me), lambda c: c.wait_send())
+        each(row_copy(1, d, me + d, me), lambda c: c.wait_send())
         return 0
 
     lax.fori_loop(1, devices - me, drain_rows, 0)
+
+    @pl.when(me < devices - 1)
+    def _():
+        for kind in range(2):
+            root_copy(kind, True).wait_send()
 
 
 def on_device(devices, tokens, query_weight, key_weight, value_weight, out_weight, chosen):
@@ -283,9 +347,11 @@
     return pl.pallas_call(
         functools.partial(layer, devices),
         out_shape=jax.ShapeDtypeStruct((rows, out_weight.shape[1]), BF16),
-        in_specs=[vmem, vmem] + [anywhere] * 6,
+        in_specs=[anywhere] * 8,
         out_specs=vmem,
         scratch_shapes=[
+            pltpu.VMEM(chosen.shape, jnp.int32),
+            pltpu.VMEM(base_table.shape, F32),
             pltpu.VMEM((rows, 2 * LANES), F32),
             pltpu.VMEM((rows, half), BF16),
             pltpu.VMEM((rows, half), BF16),
@@ -300,6 +366,7 @@
             pltpu.VMEM((rows, head_width), BF16),
             pltpu.VMEM((pairs, 2 * rows, LANES), BF16),
             pltpu.VMEM((devices,) + chosen.shape, jnp.int32),
+            pltpu.VMEM((devices, picked, rows), BF16),
             pltpu.VMEM((devices, picked, head_width), BF16),
             pltpu.VMEM((devices, picked, head_width), BF16),
             pltpu.VMEM((devices, picked, head_width), BF16),
@@ -307,15 +374,18 @@
             pltpu.VMEM((pairs, 2 * rows, 1), F32),
             pltpu.VMEM((pairs, 2 * rows, 1), F32),
             pltpu.VMEM((pairs, 2 * rows, LANES), F32),
-            pltpu.VMEM((rows, head_width), BF16),
-            pltpu.VMEM((rows, head_width), BF16),
-            dma((6,)),
+            pltpu.VMEM((pairs, 2 * rows, picked), BF16),
+            pltpu.VMEM((pairs, rows, LANES), BF16),
+            pltpu.VMEM((pairs, rows, LANES), BF16),
+            dma((8,)),
             dma((2,)),
-            dma((2,)),
+            dma((2, pairs)),
             dma((devices,)),
             dma((devices,)),
             dma((2, devices)),
             dma((2, devices)),
+            dma((2,)),
+            dma((2,)),
         ],
         compiler_params=pltpu.CompilerParams(
             collective_id=0, has_side_effects=True, vmem_limit_bytes=60 * 1024 * 1024

time: 35.2 us -> 37.6 us (1.068)
  the two profiles are of different devices: /device:TPU:17 before, /device:TPU:25 now
where the time goes in v2:
time: 37.6 us; the launch traced here: 37.5 us
  Pallas kernels  35.6 us (95%)
  local copies, waits for them, and re-layouts  1.87 us (5%)
    pallas_call x1, Pallas kernels, on_device(): pl.pallas_call(functools.partial(layer, devices), out_shape=jax.ShapeDtyp...  35.6 us
    unnamed x1, local copies, waits for them, and re-layouts  1.87 us

profile of v2, /device:TPU:25, one launch (start us, length us, event | category | flops | bytes accessed | tf_op | source)
XLA Modules:
  0.0 37.5 jit_solution(4201861686966154135)
XLA Ops:
  0.0 35.6 %layer.1 = bf16[256,1024]{1,0:T(8,128)(2,1)} custom-call(s32[8,16]{1,0:T(8,128)} %chosen_hbm.1, f32[4,256]{1,0:T(4,128)} %constant.4.clone.base_hbm, f32[256,256]{1,0:T(8,128)} %constant.5.clone.row_hbm, bf16[256,1024]{1,0:T(8,128)(2,1)} %tok_hbm.1, bf16[2048,512]{1,0:T(8,128)(2,1)} %wq_hbm.1, bf16[2048,512]{1,0:T(8,128)(2,1)} %wk_hbm.1, ...), custom_call_target="tpu_custom_call" | custom-call | tf_op jit(solution)/shard_map/layer/pallas_call | solution.py:347
  35.6 1.9 %copy.10 = bf16[256,1024]{1,0:T(8,128)(2,1)} copy(bf16[256,1024]{1,0:T(8,128)(2,1)} %layer.1) | data formatting | bytes 1048576

commit v3 on v2

--- a/solution.py
+++ b/solution.py
@@ -56,7 +56,7 @@
     chosen_hbm, base_hbm, row_hbm, tok_hbm, wq_hbm, wk_hbm, wv_hbm, wo_hbm,
     out_ref,
     chosen_ref, base_ref, tab, tok_own, tok_peer, wq, wk, wv, wo, q_acc, k_acc, v_acc, k_own, v_own, q2,
-    lists, picks, k_send, v_send, k_recv, v_recv, peak, total, summed, weigh, att_own, att_peer,
+    lists, picks, k_rows, v_rows, raw, widest, peak, total, summed, weigh, att_own, att_peer,
     load_sem, tok_sem, att_sem, list_send, list_recv, key_send, key_recv, root_send, root_recv,
 ):
     me = lax.axis_index("kv")
@@ -151,14 +151,14 @@
         tile = slice(i * LANES, (i + 1) * LANES)
         k_own[:, tile] = rotated(k_full[:, tile]).astype(BF16)
 
-    buffers = ((k_own, k_send, k_recv), (v_own, v_send, v_recv))
+    buffers = ((k_own, k_rows), (v_own, v_rows))
 
     def row_copy(kind, d, target, holder):
-        _, source, landing = buffers[kind]
+        buffer = buffers[kind][1]
 
         def part(span):
             return pltpu.make_async_remote_copy(
-                src_ref=source.at[d, span], dst_ref=landing.at[d, span],
+                src_ref=buffer.at[lax.rem(me + d, devices), span], dst_ref=buffer.at[d, span],
                 send_sem=key_send.at[kind, d], recv_sem=key_recv.at[kind, d],
                 device_id={"kv": target}, device_id_type=MESH,
             )
@@ -170,50 +170,53 @@
         pl.when(is_short)(lambda: act(short))
         pl.when(jnp.logical_not(is_short))(lambda: act(whole))
 
-    def root_copy(kind, from_own):
-        own, _, landing = buffers[kind]
-        block = slice(0, BLOCK)
-        source = own.at[block] if from_own else landing.at[me, block]
-        return pltpu.make_async_remote_copy(
-            src_ref=source, dst_ref=landing.at[lax.rem(me + 1, devices), block],
-            send_sem=root_send.at[kind], recv_sem=root_recv.at[kind],
-            device_id={"kv": lax.rem(me + 1, devices)}, device_id_type=MESH,
-        )
-
-    def root_arrival(kind):
-        landing = buffers[kind][2]
+    def root_copy(kind, d):
+        own, buffer = buffers[kind]
         block = slice(0, BLOCK)
         return pltpu.make_async_remote_copy(
-            src_ref=landing.at[me, block], dst_ref=landing.at[me, block],
-            send_sem=root_send.at[kind], recv_sem=root_recv.at[kind],
-            device_id={"kv": lax.rem(me + 1, devices)}, device_id_type=MESH,
-        )
-
-    @pl.when(me == 0)
-    def _():
-        root_copy(0, True).start()
-
-    def send_keys(d, _):
+            src_ref=own.at[block], dst_ref=buffer.at[d, block],
+            send_sem=root_send.at[kind, d], recv_sem=root_recv.at[kind],
+            device_id={"kv": lax.rem(d, devices)}, device_id_type=MESH,
+        )
+
+    def send_root(kind):
+        @pl.when(me == 0)
+        def _():
+            def one(step, _):
+                root_copy(kind, devices - 1 - step).start()
+                return 0
+
+            lax.fori_loop(0, devices - 1, one, 0)
+
+    def arrived(kind, d):
+        each(row_copy(kind, d, me, me - d), lambda c: c.wait_recv())
+
+        @pl.when(d == me)
+        def _():
+            root_copy(kind, d).wait_recv()
+
+    send_root(0)
+
+    def send_keys(step, _):
+        d = devices - 1 - me - step
         list_copy(d, me).wait_recv()
         pick = selection(listed_columns(lists[d], me, rows), earlier)
         picks[d] = pick
-        k_send[d] = jnp.dot(pick, k_own[...], preferred_element_type=F32).astype(BF16)
+        k_rows[me + d] = jnp.dot(pick, k_own[...], preferred_element_type=F32).astype(BF16)
         each(row_copy(0, d, me + d, me), lambda c: c.start())
         return 0
 
-    lax.fori_loop(1, devices - me, send_keys, 0)
+    lax.fori_loop(0, devices - 1 - me, send_keys, 0)
 
     v_own[...] = (
         v_acc[...] + jnp.dot(tok_peer[...], wv[peer_half, :], preferred_element_type=F32)
     ).astype(BF16)
 
-    @pl.when(me == 0)
-    def _():
-        root_copy(1, True).start()
+    send_root(1)
 
     def send_values(step, _):
         d = devices - 1 - me - step
-        v_send[d] = jnp.dot(picks[d], v_own[...], preferred_element_type=F32).astype(BF16)
+        v_rows[me + d] = jnp.dot(picks[d], v_own[...], preferred_element_type=F32).astype(BF16)
         each(row_copy(1, d, me + d, me), lambda c: c.start())
         return 0
 
@@ -239,16 +242,22 @@
             q2[i], keys, (((1,), (1,)), ((), ())), preferred_element_type=F32
         )
 
-    def relay(kind):
-        @pl.when(me > 0)
-        def _():
-            root_arrival(kind).wait_recv()
-
-            @pl.when(me < devices - 1)
-            def _():
-                root_copy(kind, False).start()
-
-    relay(0)
+    def gauge(d, _):
+        hit = listed_columns(chosen, me - d, rows)
+        pick = selection(hit, earlier)
+        got = lax.dot_general(
+            hit.astype(BF16), pick, (((1,), (1,)), ((), ())), preferred_element_type=F32
+        )
+        far = jnp.where(spread(got) > 0.5, 0.0, MASKED)
+        far = jnp.concatenate([far, far], axis=0)
+        arrived(0, d)
+        for i in range(pairs):
+            tile = slice(i * LANES, (i + 1) * LANES)
+            scores = scores_of(i, k_rows[d, :, tile]) + far
+            raw[d - 1, i] = scores
+            widest[i] = jnp.maximum(widest[i], scores)
+        return 0
+
     listed = spread(listed_columns(chosen, me, rows))
     bias = jnp.where((listed > 0.5) & (col_i <= row_i), 0.0, MASKED)
     bias = jnp.concatenate([bias, bias], axis=0)
@@ -257,43 +266,40 @@
         scores = scores_of(i, k_own[:, tile]) + bias
         top = jnp.max(scores, axis=1, keepdims=True)
         weights = jnp.exp(scores - top)
-        peak[i] = top
-        total[i] = jnp.sum(weights, axis=1, keepdims=True)
+        peak[i] = jnp.broadcast_to(top, peak.shape[1:])
+        total[i] = sum(weights[:, j : j + LANES] for j in range(0, rows, LANES))
         summed[i] = jnp.dot(weights.astype(BF16), v_own[:, tile], preferred_element_type=F32)
-    relay(1)
+        widest[i] = jnp.full(widest.shape[1:], MASKED, F32)
+
+    lax.fori_loop(1, me + 1, gauge, 0)
+
+    @pl.when(me > 0)
+    def _():
+        for i in range(pairs):
+            old = peak[i]
+            top = jnp.maximum(old, jnp.max(widest[i], axis=1, keepdims=True))
+            factor = jnp.exp(old - top)
+            peak[i] = top
+            total[i] = total[i] * factor
+            summed[i] = summed[i] * factor
 
     def attend(step, _):
         d = jnp.where(me == devices - 1, step, me + 1 - step)
-        hit = listed_columns(chosen, me - d, rows)
-        pick = selection(hit, earlier)
-        got = lax.dot_general(
-            hit.astype(BF16), pick, (((1,), (1,)), ((), ())), preferred_element_type=F32
-        )
-        far = jnp.where(spread(got) > 0.5, 0.0, MASKED)
-        far = jnp.concatenate([far, far], axis=0)
-        each(row_copy(0, d, me, me - d), lambda c: c.wait_recv())
+        for i in range(pairs):
+            weights = jnp.exp(raw[d - 1, i] - peak[i, :, :picked])
+            total[i, :, :picked] += weights
+            weigh[i] = weights.astype(BF16)
+        arrived(1, d)
         for i in range(pairs):
             tile = slice(i * LANES, (i + 1) * LANES)
-            scores = scores_of(i, k_recv[d, :, tile]) + far
-            old = peak[i]
-            top = jnp.maximum(old, jnp.max(scores, axis=1, keepdims=True))
-            factor = jnp.exp(old - top)
-            weights = jnp.exp(scores - top)
-            peak[i] = top
-            total[i] = total[i] * factor + jnp.sum(weights, axis=1, keepdims=True)
-            summed[i] = summed[i] * factor
-            weigh[i] = weights.astype(BF16)
-        each(row_copy(1, d, me, me - d), lambda c: c.wait_recv())
-        for i in range(pairs):
-            tile = slice(i * LANES, (i + 1) * LANES)
-            summed[i] += jnp.dot(weigh[i], v_recv[d, :, tile], preferred_element_type=F32)
+            summed[i] += jnp.dot(weigh[i], v_rows[d, :, tile], preferred_element_type=F32)
         return 0
 
     lax.fori_loop(1, me + 1, attend, 0)
 
     att_copies = []
     for i in range(pairs):
-        ratio = summed[i] / total[i]
+        ratio = summed[i] / jnp.sum(total[i], axis=1, keepdims=True)
         att_own[i] = jnp.where(lane < HEAD_DIM, ratio[:rows], ratio[rows:]).astype(BF16)
         att_copies.append(
             pltpu.make_async_remote_copy(
@@ -329,10 +335,14 @@
 
     lax.fori_loop(1, devices - me, drain_rows, 0)
 
-    @pl.when(me < devices - 1)
+    @pl.when(me == 0)
     def _():
-        for kind in range(2):
-            root_copy(kind, True).wait_send()
+        def drain_root(d, _):
+            root_copy(0, d).wait_send()
+            root_copy(1, d).wait_send()
+            return 0
+
+        lax.fori_loop(1, devices, drain_root, 0)
 
 
 def on_device(devices, tokens, query_weight, key_weight, value_weight, out_weight, chosen):
@@ -346,7 +356,7 @@
     dma = pltpu.SemaphoreType.DMA
     return pl.pallas_call(
         functools.partial(layer, devices),
-        out_shape=jax.ShapeDtypeStruct((rows, out_weight.shape[1]), BF16),
+        out_shape=pltpu.VMEM((rows, out_weight.shape[1]), BF16),
         in_specs=[anywhere] * 8,
         out_specs=vmem,
         scratch_shapes=[
@@ -369,10 +379,10 @@
             pltpu.VMEM((devices, picked, rows), BF16),
             pltpu.VMEM((devices, picked, head_width), BF16),
             pltpu.VMEM((devices, picked, head_width), BF16),
-            pltpu.VMEM((devices, picked, head_width), BF16),
-            pltpu.VMEM((devices, picked, head_width), BF16),
-            pltpu.VMEM((pairs, 2 * rows, 1), F32),
-            pltpu.VMEM((pairs, 2 * rows, 1), F32),
+            pltpu.VMEM((devices - 1, pairs, 2 * rows, picked), F32),
+            pltpu.VMEM((pairs, 2 * rows, picked), F32),
+            pltpu.VMEM((pairs, 2 * rows, LANES), F32),
+            pltpu.VMEM((pairs, 2 * rows, LANES), F32),
             pltpu.VMEM((pairs, 2 * rows, LANES), F32),
             pltpu.VMEM((pairs, 2 * rows, picked), BF16),
             pltpu.VMEM((pairs, rows, LANES), BF16),
@@ -384,11 +394,11 @@
             dma((devices,)),
             dma((2, devices)),
             dma((2, devices)),
-            dma((2,)),
+            dma((2, devices)),
             dma((2,)),
         ],
         compiler_params=pltpu.CompilerParams(
-            collective_id=0, has_side_effects=True, vmem_limit_bytes=60 * 1024 * 1024
+            collective_id=0, has_side_effects=True, vmem_limit_bytes=62 * 1024 * 1024
         ),
         name="layer",
     )(

time: 37.6 us -> 28.4 us (0.76)
  the two profiles are of different devices: /device:TPU:25 before, /device:TPU:17 now
where the time goes in v3:
time: 28.4 us; the launch traced here: 28.3 us
  Pallas kernels  27.4 us (96%)
  local copies, waits for them, and re-layouts  0.8 us (3%)
    pallas_call x1, Pallas kernels, on_device(): pl.pallas_call(functools.partial(layer, devices), out_shape=pltpu.VMEM((r...  27.4 us
    unnamed x1, local copies, waits for them, and re-layouts  0.8 us

profile of v3, /device:TPU:17, one launch (start us, length us, event | category | flops | bytes accessed | tf_op | source)
XLA Modules:
  0.0 28.3 jit_solution(15371693568241429434)
XLA Ops:
  0.0 27.4 %layer.1 = bf16[256,1024]{1,0:T(8,128)(2,1)S(1)} custom-call(s32[8,16]{1,0:T(8,128)} %chosen_hbm.1, f32[4,256]{1,0:T(4,128)} %constant.4.clone.base_hbm, f32[256,256]{1,0:T(8,128)} %constant.5.clone.row_hbm, bf16[256,1024]{1,0:T(8,128)(2,1)} %tok_hbm.1, bf16[2048,512]{1,0:T(8,128)(2,1)} %wq_hbm.1, bf16[2048,512]{1,0:T(8,128)(2,1)} %wk_hbm.1, ...), custom_call_target="tpu_custom_call" | custom-call | tf_op jit(solution)/shard_map/layer/pallas_call | solution.py:357
  27.5 0.8 %copy.10 = bf16[256,1024]{1,0:T(8,128)(2,1)} copy(bf16[256,1024]{1,0:T(8,128)(2,1)S(1)} %layer.1) | data formatting | bytes 1048576

commit v4 on v3

--- a/solution.py
+++ b/solution.py
@@ -170,11 +170,15 @@
         pl.when(is_short)(lambda: act(short))
         pl.when(jnp.logical_not(is_short))(lambda: act(whole))
 
-    def root_copy(kind, d):
+    relayed = devices > 2
+    direct = devices - 2 if relayed else devices - 1
+    relay_here = (me == devices - 2) if relayed else False
+
+    def root_copy(kind, d, passing=False):
         own, buffer = buffers[kind]
         block = slice(0, BLOCK)
         return pltpu.make_async_remote_copy(
-            src_ref=own.at[block], dst_ref=buffer.at[d, block],
+            src_ref=buffer.at[me, block] if passing else own.at[block], dst_ref=buffer.at[d, block],
             send_sem=root_send.at[kind, d], recv_sem=root_recv.at[kind],
             device_id={"kv": lax.rem(d, devices)}, device_id_type=MESH,
         )
@@ -183,22 +187,21 @@
         @pl.when(me == 0)
         def _():
             def one(step, _):
-                root_copy(kind, devices - 1 - step).start()
+                root_copy(kind, direct - step).start()
                 return 0
 
-            lax.fori_loop(0, devices - 1, one, 0)
+            lax.fori_loop(0, direct, one, 0)
 
     def arrived(kind, d):
         each(row_copy(kind, d, me, me - d), lambda c: c.wait_recv())
 
-        @pl.when(d == me)
+        @pl.when((d == me) & jnp.logical_not(relay_here))
         def _():
             root_copy(kind, d).wait_recv()
 
     send_root(0)
 
-    def send_keys(step, _):
-        d = devices - 1 - me - step
+    def send_keys(d, _):
         list_copy(d, me).wait_recv()
         pick = selection(listed_columns(lists[d], me, rows), earlier)
         picks[d] = pick
@@ -206,7 +209,7 @@
         each(row_copy(0, d, me + d, me), lambda c: c.start())
         return 0
 
-    lax.fori_loop(0, devices - 1 - me, send_keys, 0)
+    lax.fori_loop(1, devices - me, send_keys, 0)
 
     v_own[...] = (
         v_acc[...] + jnp.dot(tok_peer[...], wv[peer_half, :], preferred_element_type=F32)
@@ -271,6 +274,14 @@
         summed[i] = jnp.dot(weights.astype(BF16), v_own[:, tile], preferred_element_type=F32)
         widest[i] = jnp.full(widest.shape[1:], MASKED, F32)
 
+    if relayed:
+
+        @pl.when(relay_here)
+        def _():
+            for kind in range(2):
+                root_copy(kind, me).wait_recv()
+                root_copy(kind, devices - 1, True).start()
+
     lax.fori_loop(1, me + 1, gauge, 0)
 
     @pl.when(me > 0)
@@ -342,7 +353,14 @@
             root_copy(1, d).wait_send()
             return 0
 
-        lax.fori_loop(1, devices, drain_root, 0)
+        lax.fori_loop(1, direct + 1, drain_root, 0)
+
+    if relayed:
+
+        @pl.when(relay_here)
+        def _():
+            for kind in range(2):
+                root_copy(kind, devices - 1, True).wait_send()
 
 
 def on_device(devices, tokens, query_weight, key_weight, value_weight, out_weight, chosen):

time: 28.4 us -> 26.8 us (0.944)
  Pallas kernels: 27.4 us -> 25.9 us
    pallas_call x1, Pallas kernels: 27.4 us -> 25.9 us  [on_device(): pl.pallas_call(functools.partial(layer, devices), out_shape=pltpu.VMEM((r...]
where the time goes in v4:
time: 26.8 us; the launch traced here: 26.7 us
  Pallas kernels  25.9 us (97%)
  local copies, waits for them, and re-layouts  0.8 us (3%)
    pallas_call x1, Pallas kernels, on_device(): pl.pallas_call(functools.partial(layer, devices), out_shape=pltpu.VMEM((r...  25.9 us
    unnamed x1, local copies, waits for them, and re-layouts  0.8 us

profile of v4, /device:TPU:17, one launch (start us, length us, event | category | flops | bytes accessed | tf_op | source)
XLA Modules:
  0.0 26.7 jit_solution(3026065839966293015)
XLA Ops:
  0.0 25.9 %layer.1 = bf16[256,1024]{1,0:T(8,128)(2,1)S(1)} custom-call(s32[8,16]{1,0:T(8,128)} %chosen_hbm.1, f32[4,256]{1,0:T(4,128)} %constant.4.clone.base_hbm, f32[256,256]{1,0:T(8,128)} %constant.5.clone.row_hbm, bf16[256,1024]{1,0:T(8,128)(2,1)} %tok_hbm.1, bf16[2048,512]{1,0:T(8,128)(2,1)} %wq_hbm.1, bf16[2048,512]{1,0:T(8,128)(2,1)} %wk_hbm.1, ...), custom_call_target="tpu_custom_call" | custom-call | tf_op jit(solution)/shard_map/layer/pallas_call | solution.py:375
  25.9 0.8 %copy.10 = bf16[256,1024]{1,0:T(8,128)(2,1)} copy(bf16[256,1024]{1,0:T(8,128)(2,1)S(1)} %layer.1) | data formatting | bytes 1048576
